TPU v7x, 32 devices: a whole 2x2x4 slice. The times are simulated.
32 devices in a mesh: grp: 2 (over y), sp: 4 (over z), tp: 4 (over x, core).
Axes of the slice: x: 2, y: 2, z: 4, core: 2. Of those that a mesh axis runs over, the one named last changes fastest.
Arguments:
- query_nope: bfloat16 [2560, 1024], P(('grp', 'sp'), 'tp'), parts along dimension 0, may hold values from -12 to 12
- query_rope: bfloat16 [2560, 512], P(('grp', 'sp'), 'tp'), parts along dimension 0, may hold values from -48 to 48
- token_latent: bfloat16 [2560, 256], P(('grp', 'sp')), parts along dimension 0, may hold values from -6 to 6
- key_rope: bfloat16 [2560, 32], P(('grp', 'sp')), parts along dimension 0, may hold values from -48 to 48
- latent_norm_gain: float32 [256], replicated, may hold values from 0.1 to 1.9
- key_expand_weight: bfloat16 [256, 1024], replicated, may hold values from -0.375 to 0.375
- value_expand_weight: bfloat16 [256, 1024], replicated, may hold values from -0.375 to 0.375
- residual: bfloat16 [2560, 2048], P(('grp', 'sp')), parts along dimension 0, may hold values from -3 to 3
- out_weight: bfloat16 [1024, 2048], P('tp'), may hold values from -0.375 to 0.375
- ffn_gain: float32 [2048], replicated, may hold values from 0.1 to 1.9
- gate_weight: bfloat16 [2048, 5632], P('sp', 'tp'), may hold values from -0.125 to 0.125
- up_weight: bfloat16 [2048, 5632], P('sp', 'tp'), may hold values from -0.125 to 0.125
- down_weight: bfloat16 [5632, 2048], P('tp', 'sp'), may hold values from -0.078125 to 0.078125
Outputs:
- layer_output: bfloat16 [2560, 2048], P(('grp', 'sp', 'tp')), parts along dimension 0
There are 2 independent parts, one for each index of `grp`. A program takes and returns all parts, laid end to end along the dimension named above; an argument that names none is the same for every part. Nothing has to cross between parts.
All inputs are finite; a program needn't handle non-finite values.
Results may differ from a plain program's by a relative error of at most 0.015.
Values may be sent and summed in bfloat16 or wider, within the bound.
A program may use at most 128 MiB of HBM per device.

v0:
```python
import functools

import jax
import jax.numpy as jnp
from jax import lax
from jax.experimental import pallas as pl
from jax.experimental.pallas import tpu as pltpu
from jax.sharding import PartitionSpec as P

MESH = pl.DeviceIdType.MESH
UNROTATED_SIZE = 64
ROPE = 32
VALUE_SIZE = 64
GRID_W = 64


def norm_rows(values, gain):
    wide = values.astype(jnp.float32)
    return wide * lax.rsqrt(jnp.mean(wide * wide, axis=-1, keepdims=True) + 1e-06) * gain


def turn_heads(vectors, positions):
    tokens, heads, width = vectors.shape
    freqs = width // 4
    grid_pos = jnp.stack([positions // GRID_W, positions % GRID_W], axis=-1).astype(jnp.float32)
    inverse = jnp.power(10000.0, -jnp.arange(freqs, dtype=jnp.float32) / freqs)
    angles = grid_pos[:, :, None] * inverse
    cosine = jnp.cos(angles)[:, None]
    sine = jnp.sin(angles)[:, None]
    viewed = vectors.reshape(tokens, heads, 2, 2, freqs)
    first = viewed[..., 0, :]
    second = viewed[..., 1, :]
    turned = jnp.stack([first * cosine - second * sine, first * sine + second * cosine], axis=-2)
    return turned.reshape(tokens, heads, width)


def spread_hidden(token_count, hidden_columns):
    fits = lax.axis_size("tp") == 4 and lax.axis_size("grp") == 2
    return fits and 2 * token_count < 3 * hidden_columns


def column_tiles(hidden_columns):
    tiles = hidden_columns // 128
    return tiles, -(-tiles // lax.axis_size("sp"))


def window_start(at, hidden_columns):
    tiles, per = column_tiles(hidden_columns)
    return lax.div(at * (tiles - per), lax.axis_size("sp") - 1)


def signal_all(peers):
    barrier = pltpu.get_barrier_semaphore()
    for peer in peers:
        pl.semaphore_signal(barrier, inc=1, device_id=peer, device_id_type=MESH)
    pl.semaphore_wait(barrier, len(peers))


def remote(src, dst, send_sem, recv_sem, peer):
    return pltpu.make_async_remote_copy(
        src_ref=src,
        dst_ref=dst,
        send_sem=send_sem,
        recv_sem=recv_sem,
        device_id=peer,
        device_id_type=MESH,
    )


def front_kernel(
    size, hidden_columns, query, turned, latent, key_w, value_w, out_w, residual, gain,
    gate, up, down,
    gate_out, up_out, down_out, mixed, normed,
    gathered, projected, landed,
    own_sem, z_send, z_recv, y_send, y_recv, l_send, l_recv, m_send, m_recv, r_send, r_recv,
):
    here = lax.axis_index("sp")
    part = lax.axis_index("grp")
    t = lax.axis_index("tp")
    side = lax.rem(t, 2)
    core = t + 1 - 2 * side
    depth = gate.shape[0]
    width = gate_out.shape[1]
    outer = down.shape[1]

    def start_of(at):
        return pl.multiple_of(window_start(at, hidden_columns) * 128, 128)

    def piece(out, kind, origin, half):
        if kind < 2:
            rows = depth // 2
            return out.at[pl.ds(pl.multiple_of(origin * depth + half * rows, rows), rows), :]
        rows = width // 2
        return out.at[
            pl.ds(pl.multiple_of(half * rows, rows), rows),
            pl.ds(pl.multiple_of(origin * outer, outer), outer),
        ]

    def source(ref, kind, target, half):
        if kind < 2:
            rows = depth // 2
            return ref.at[pl.ds(pl.multiple_of(half * rows, rows), rows), pl.ds(start_of(target), width)]
        rows = width // 2
        return ref.at[pl.ds(pl.multiple_of(start_of(target) + half * rows, 64), rows), :]

    peers = [{"sp": lax.rem(here + shift, size)} for shift in range(1, size)]
    peers += [{"tp": lax.rem(t + shift, 4)} for shift in range(1, 4)]
    signal_all(peers + [{"grp": 1 - part}])
    tokens = latent.shape[0]
    half_rows = tokens // 2
    my_half = pl.ds(pl.multiple_of(side * half_rows, half_rows), half_rows)
    spread_latent = []
    for shift in range(1, size):
        copy = remote(
            latent.at[my_half, :],
            gathered.at[here, my_half, :],
            l_send.at[shift - 1],
            l_recv.at[shift - 1],
            {"sp": lax.rem(here + shift, size)},
        )
        copy.start()
        spread_latent.append(copy)
    refs = ((gate, gate_out), (up, up_out), (down, down_out))
    across = []
    for kind, (ref, out) in enumerate(refs):
        for shift in range(1, size):
            target = lax.rem(here + shift, size)
            copy = remote(
                source(ref, kind, target, part),
                piece(out, kind, here, part),
                z_send.at[kind, shift - 1],
                z_recv.at[kind, shift - 1],
                {"sp": target},
            )
            copy.start()
            across.append(copy)
    locals_ = []
    for kind, (ref, out) in enumerate(refs):
        for half in range(2):
            copy = pltpu.make_async_copy(
                source(ref, kind, here, half), piece(out, kind, here, half), own_sem.at[kind, half]
            )
            copy.start()
            locals_.append(copy)
    gathered[here] = latent[...]
    shared_latent = []
    for shift in range(1, size):
        spread_latent[shift - 1].wait_recv()
        held = gathered.at[lax.rem(here - shift + size, size), my_half, :]
        copy = remote(held, held, m_send.at[shift - 1], m_recv.at[shift - 1], {"tp": core})
        copy.start()
        shared_latent.append(copy)
    for copy in shared_latent:
        copy.wait_recv()

    lanes = query.shape[1]
    heads = lanes // UNROTATED_SIZE
    rank = key_w.shape[0]
    columns = pl.ds(pl.multiple_of(t * lanes, 128), lanes)
    every = gathered[...].reshape(size * tokens, latent.shape[1])
    every_latent = every[:, :rank]
    keys = jnp.dot(every_latent, key_w[:, columns], preferred_element_type=jnp.float32)
    values = jnp.dot(every_latent, value_w[:, columns], preferred_element_type=jnp.float32)
    values = values.astype(jnp.bfloat16)
    keys = jnp.concatenate([keys.astype(jnp.bfloat16), every[:, rank:]], axis=1)
    scale = (UNROTATED_SIZE + ROPE) ** (-0.5)
    lane = lax.broadcasted_iota(jnp.int32, (1, lanes), 1)
    rope_lane = lax.broadcasted_iota(jnp.int32, (1, turned.shape[1]), 1)
    attended = jnp.zeros((tokens, lanes), jnp.float32)
    for head in range(heads):
        mine = (lane >= head * UNROTATED_SIZE) & (lane < (head + 1) * UNROTATED_SIZE)
        rope_mine = (rope_lane >= head * ROPE) & (rope_lane < (head + 1) * ROPE)
        both = jnp.concatenate(
            [
                jnp.where(mine, query[...].astype(jnp.float32), 0.0),
                jnp.where(rope_mine, turned[...].astype(jnp.float32), 0.0),
            ],
            axis=1,
        ).astype(jnp.bfloat16)
        scores = (
            lax.dot_general(
                both, keys, (((1,), (1,)), ((), ())), preferred_element_type=jnp.float32
            )
            * scale
        )
        raised = jnp.exp(scores - jnp.max(scores, axis=1, keepdims=True))
        totals = jnp.sum(raised, axis=1, keepdims=True)
        weighted = jnp.dot(
            raised.astype(jnp.bfloat16), values, preferred_element_type=jnp.float32
        )
        attended = jnp.where(mine, weighted / totals, attended)
    attended = attended.astype(jnp.bfloat16)
    own_rows = mixed.shape[0]
    step = 512
    for col in range(0, out_w.shape[1], step):
        term = jnp.dot(
            attended, out_w[:, col : col + step], preferred_element_type=jnp.float32
        )
        projected[:, :, col : col + step] = term.astype(jnp.bfloat16).reshape(4, own_rows, step)
    scattered = []
    for shift in (2, 1, 3):
        target = lax.rem(t + shift, 4)
        copy = remote(
            projected.at[target],
            landed.at[shift - 1],
            r_send.at[shift - 1],
            r_recv.at[shift - 1],
            {"tp": target},
        )
        copy.start()
        scattered.append(copy)

    swaps = []

    def forward(kind):
        out = refs[kind][1]
        for shift in range(1, size):
            origin = lax.rem(here - shift + size, size)
            across[kind * (size - 1) + shift - 1].wait_recv()
            held = piece(out, kind, origin, part)
            copy = remote(
                held, held, y_send.at[kind, shift - 1], y_recv.at[kind, shift - 1], {"grp": 1 - part}
            )
            copy.start()
            swaps.append(copy)

    forward(0)
    forward(1)
    for copy in scattered:
        copy.wait_recv()
    rows = pl.ds(pl.multiple_of(t * own_rows, own_rows), own_rows)
    total = residual[rows, :].astype(jnp.float32) + projected[t].astype(jnp.float32)
    for shift in range(3):
        total = total + landed[shift].astype(jnp.float32)
    mixed[...] = total
    normed[...] = (
        total * lax.rsqrt(jnp.mean(total * total, axis=1, keepdims=True) + 1e-06) * gain[...]
    ).astype(jnp.bfloat16)
    forward(2)
    for copy in across + spread_latent + shared_latent + scattered:
        copy.wait_send()
    for copy in locals_:
        copy.wait()
    for copy in swaps:
        copy.wait()


def front(query, turned, latent, key_w, value_w, out_w, residual, gain, gate, up, down):
    size = lax.axis_size("sp")
    depth, columns = gate.shape
    width = column_tiles(columns)[1] * 128
    own = (residual.shape[0] // lax.axis_size("tp"), residual.shape[1])
    wide = jax.ShapeDtypeStruct((size * depth, width), gate.dtype)
    tall = jax.ShapeDtypeStruct((width, size * down.shape[1]), down.dtype)
    dma = pltpu.SemaphoreType.DMA
    pairs = dma((3, size - 1))
    line = dma((size - 1,))
    here = pl.BlockSpec(memory_space=pltpu.VMEM)
    away = pl.BlockSpec(memory_space=pl.ANY)
    return pl.pallas_call(
        functools.partial(front_kernel, size, columns),
        out_shape=(
            wide, wide, tall,
            jax.ShapeDtypeStruct(own, jnp.float32), jax.ShapeDtypeStruct(own, jnp.bfloat16),
        ),
        in_specs=[here] * 8 + [away] * 3,
        out_specs=[away] * 3 + [here] * 2,
        scratch_shapes=[
            pltpu.VMEM((size,) + latent.shape, jnp.bfloat16),
            pltpu.VMEM((4,) + own, jnp.bfloat16),
            pltpu.VMEM((3,) + own, jnp.bfloat16),
            dma((3, 2)), pairs, pairs, pairs, pairs, line, line, line, line, dma((3,)), dma((3,)),
        ],
        compiler_params=pltpu.CompilerParams(collective_id=0, has_side_effects=True),
        name="front",
    )(query, turned, latent, key_w, value_w, out_w, residual, gain, gate, up, down)


def turn_lanes(vectors, positions):
    lanes = vectors.shape[1]
    freqs = ROPE // 4
    lane = jnp.arange(lanes, dtype=jnp.int32)
    inverse = jnp.power(10000.0, -(lane % freqs).astype(jnp.float32) / freqs)
    first_axis = lane % ROPE < ROPE // 2
    first_half = lane % (2 * freqs) < freqs
    place = jnp.where(
        first_axis[None], (positions // GRID_W)[:, None], (positions % GRID_W)[:, None]
    )
    angles = place.astype(jnp.float32) * inverse[None]
    partner = jnp.where(first_half, lane + freqs, lane - freqs)
    sign = jnp.where(first_half, -1.0, 1.0)
    swap = jnp.where(lane[:, None] == partner[None], sign[None], 0.0).astype(vectors.dtype)
    other = jnp.dot(vectors, swap, preferred_element_type=jnp.float32)
    turned = vectors.astype(jnp.float32) * jnp.cos(angles) + other * jnp.sin(angles)
    return turned.astype(jnp.bfloat16)


def spread_layer(
    query_nope, query_rope, token_latent, key_rope, latent_norm_gain, key_w, value_w,
    residual, out_w, ffn_gain, gate_w, up_w, down_w,
):
    rows = query_nope.shape[0]
    positions = lax.axis_index("sp") * rows + jnp.arange(rows, dtype=jnp.int32)
    repeats = query_rope.shape[1] // ROPE
    turned = turn_lanes(query_rope, positions)
    key_turned = turn_lanes(jnp.tile(key_rope, (1, repeats)), positions)
    latent = norm_rows(token_latent, latent_norm_gain).astype(jnp.bfloat16)
    packed = jnp.concatenate([latent, key_turned], axis=1)
    gate, up, down, mixed, normed = front(
        query_nope, turned, packed, key_w, value_w, out_w, residual, ffn_gain[None],
        gate_w, up_w, down_w,
    )
    return spread_ffn(normed, mixed, (gate, up, down), gate_w.shape[1])


def ffn_kernel(
    size, own, gate_w, up_w, down_w, keep, mixed, out,
    tokens, parts, from_core, from_x, from_z, total,
    z_send, z_recv, x_send, x_recv, c_send, c_recv,
    rc_send, rc_recv, rx_send, rx_recv, rz_send, rz_recv,
):
    here = lax.axis_index("sp")
    t = lax.axis_index("tp")
    core = t + 1 - 2 * lax.rem(t, 2)
    across = t + 2 - 4 * lax.div(t, 2)
    diagonal = core + 2 - 4 * lax.div(core, 2)
    rows = own.shape[0]
    to_core, to_x = {"tp": core}, {"tp": across}
    signal_all(
        [{"sp": lax.rem(here + shift, size)} for shift in range(1, size)] + [to_core, to_x]
    )
    z_copies = [None]
    for shift in range(1, size):
        copy = remote(
            own,
            tokens.at[here, t],
            z_send.at[shift],
            z_recv.at[shift],
            {"sp": lax.rem(here + shift, size)},
        )
        copy.start()
        z_copies.append(copy)
    tokens[here, t] = own[...]
    origins = [lax.rem(here - i + size, size) for i in range(size)]
    pending = []
    x_copies, c_first, c_second, r_first, r_second, rx, rz = {}, {}, {}, {}, {}, {}, {}

    def start(table, i, *args):
        copy = remote(*args)
        copy.start()
        table[i] = copy
        pending.append(copy)

    def step_a(i):
        o = origins[i]
        if i:
            z_copies[i].wait_recv()
        block = tokens.at[o, t] if i else own
        start(x_copies, i, block, tokens.at[o, t], x_send.at[i], x_recv.at[i], to_x)
        start(c_first, i, block, tokens.at[o, t], c_send.at[i, 0], c_recv.at[i, 0], to_core)

    def step_b(i):
        o = origins[i]
        x_copies[i].wait_recv()
        block = tokens.at[o, across]
        start(c_second, i, block, block, c_send.at[i, 1], c_recv.at[i, 1], to_core)

    def step_c(i):
        o = origins[i]
        c_first[i].wait_recv()
        c_second[i].wait_recv()
        x = tokens[o].reshape(4 * rows, own.shape[1])
        gate = jnp.dot(x, gate_w[...], preferred_element_type=jnp.float32)
        up = jnp.dot(x, up_w[...], preferred_element_type=jnp.float32)
        hidden = (gate / (1.0 + jnp.exp(-gate)) * up * keep[...]).astype(jnp.bfloat16)
        step = 512
        for col in range(0, own.shape[1], step):
            term = jnp.dot(
                hidden, down_w[:, col : col + step], preferred_element_type=jnp.float32
            )
            parts[o, :, :, col : col + step] = term.astype(jnp.bfloat16).reshape(4, rows, step)
        start(r_first, i, parts.at[o, diagonal], from_core.at[i, 1], rc_send.at[i, 1], rc_recv.at[i, 1], to_core)
        start(r_second, i, parts.at[o, core], from_core.at[i, 0], rc_send.at[i, 0], rc_recv.at[i, 0], to_core)

    def plus(one, two):
        return one.astype(jnp.float32) + two.astype(jnp.float32)

    def step_d(i):
        o = origins[i]
        r_first[i].wait_recv()
        parts[o, across] = plus(parts[o, across], from_core[i, 1]).astype(jnp.bfloat16)
        start(rx, i, parts.at[o, across], from_x.at[i], rx_send.at[i], rx_recv.at[i], to_x)
        r_second[i].wait_recv()
        parts[o, t] = plus(parts[o, t], from_core[i, 0]).astype(jnp.bfloat16)

    def step_e(i):
        o = origins[i]
        rx[i].wait_recv()
        if i == 0:
            total[...] = mixed[...] + plus(parts[o, t], from_x[i])
            return
        parts[o, t] = plus(parts[o, t], from_x[i]).astype(jnp.bfloat16)
        start(rz, i, parts.at[o, t], from_z.at[i], rz_send.at[i], rz_recv.at[i], {"sp": o})

    steps = {"a": step_a, "b": step_b, "c": step_c, "d": step_d, "e": step_e}
    last = size - 1
    order = [("a", 0)]
    for i in range(size + 1):
        for name, lag in (("a", -1), ("b", 0), ("c", 0), ("d", 0), ("e", 1)):
            if 0 <= i - lag <= last:
                order.append((name, i - lag))
    for name, i in order:
        steps[name](i)
    result = total[...]
    for i in range(1, size):
        rz[i].wait_recv()
        result = result + from_z[i].astype(jnp.float32)
    out[...] = result.astype(out.dtype)
    for copy in z_copies[1:] + pending:
        copy.wait_send()


def spread_ffn(normed_own, mixed_own, swapped, hidden_columns):
    size = lax.axis_size("sp")
    here = lax.axis_index("sp")
    per = column_tiles(hidden_columns)[1]
    before = jnp.where(here > 0, window_start(jnp.maximum(here - 1, 0), hidden_columns) + per, 0)
    first = (before - window_start(here, hidden_columns)) * 128
    keep = (jnp.arange(per * 128, dtype=jnp.int32) >= first).astype(jnp.float32)[None]
    block = normed_own.shape
    dma = pltpu.SemaphoreType.DMA
    vmem = lambda *lead: pltpu.VMEM(lead + block, jnp.bfloat16)
    pair = [dma((size,)), dma((size,))]
    double = [dma((size, 2)), dma((size, 2))]
    return pl.pallas_call(
        functools.partial(ffn_kernel, size),
        out_shape=jax.ShapeDtypeStruct(block, jnp.bfloat16),
        in_specs=[pl.BlockSpec(memory_space=pltpu.VMEM)] * 6,
        out_specs=pl.BlockSpec(memory_space=pltpu.VMEM),
        scratch_shapes=[
            vmem(size, 4), vmem(size, 4), vmem(size, 2), vmem(size), vmem(size),
            pltpu.VMEM(block, jnp.float32),
        ] + pair + pair + double + double + pair + pair,
        compiler_params=pltpu.CompilerParams(collective_id=1, has_side_effects=True),
        name="spread_ffn",
    )(normed_own, *swapped, keep, mixed_own)


def local(
    query_nope,
    query_rope,
    token_latent,
    key_rope,
    latent_norm_gain,
    key_expand_weight,
    value_expand_weight,
    residual,
    out_weight,
    ffn_gain,
    gate_weight,
    up_weight,
    down_weight,
):
    if spread_hidden(query_nope.shape[0] * lax.axis_size("sp"), gate_weight.shape[1]):
        return spread_layer(
            query_nope,
            query_rope,
            token_latent,
            key_rope,
            latent_norm_gain,
            key_expand_weight,
            value_expand_weight,
            residual,
            out_weight,
            ffn_gain,
            gate_weight,
            up_weight,
            down_weight,
        )
    tok_rows = query_nope.shape[0]
    heads_here = query_nope.shape[1] // UNROTATED_SIZE
    own_rows = tok_rows // lax.axis_size("tp")
    tp_index = lax.axis_index("tp")
    positions = lax.axis_index("sp") * tok_rows + jnp.arange(tok_rows, dtype=jnp.int32)
    query_flat = query_nope.reshape(tok_rows, heads_here, UNROTATED_SIZE)
    query_turned = turn_heads(
        query_rope.astype(jnp.float32).reshape(tok_rows, heads_here, ROPE), positions
    ).astype(jnp.bfloat16)
    latent = norm_rows(token_latent, latent_norm_gain).astype(jnp.bfloat16)
    key_turned = turn_heads(key_rope.astype(jnp.float32)[:, None, :], positions)[:, 0].astype(
        jnp.bfloat16
    )
    key_cols = lax.dynamic_slice_in_dim(
        key_expand_weight, tp_index * heads_here * UNROTATED_SIZE, heads_here * UNROTATED_SIZE, 1
    )
    value_cols = lax.dynamic_slice_in_dim(
        value_expand_weight, tp_index * heads_here * VALUE_SIZE, heads_here * VALUE_SIZE, 1
    )
    score_scale = (UNROTATED_SIZE + ROPE) ** (-0.5)

    def absorb(carried, block_in):
        latent_block, rope_block = block_in
        block_rows = latent_block.shape[0]
        key_rows = jnp.dot(latent_block, key_cols, preferred_element_type=jnp.float32).astype(
            jnp.bfloat16
        )
        key_rows = key_rows.reshape(block_rows, heads_here, UNROTATED_SIZE)
        value_rows = jnp.dot(latent_block, value_cols, preferred_element_type=jnp.float32).astype(
            jnp.bfloat16
        )
        value_rows = value_rows.reshape(block_rows, heads_here, VALUE_SIZE)
        scores = (
            jnp.einsum("qhd,khd->hqk", query_flat, key_rows, preferred_element_type=jnp.float32)
            + jnp.einsum(
                "qhd,kd->hqk", query_turned, rope_block, preferred_element_type=jnp.float32
            )
        ) * score_scale
        highest, totals, accumulated = carried
        new_highest = jnp.maximum(highest, jnp.max(scores, axis=-1))
        shrink = jnp.exp(highest - new_highest)
        weights = jnp.exp(scores - new_highest[:, :, None])
        totals = totals * shrink + jnp.sum(weights, axis=-1)
        accumulated = accumulated * shrink.T[:, :, None] + jnp.einsum(
            "hqk,khd->qhd",
            weights.astype(jnp.bfloat16),
            value_rows,
            preferred_element_type=jnp.float32,
        )
        return ((new_highest, totals, accumulated), None)

    initial = (
        jnp.full((heads_here, tok_rows), -jnp.inf, jnp.float32),
        jnp.zeros((heads_here, tok_rows), jnp.float32),
        jnp.zeros((tok_rows, heads_here, VALUE_SIZE), jnp.float32),
    )
    carried = initial
    latent_piece = lax.all_gather(latent, "sp", axis=0, tiled=True)
    rope_piece = lax.all_gather(key_turned, "sp", axis=0, tiled=True)
    shard_count = latent_piece.shape[0] // tok_rows
    grouped = max(
        (
            factor
            for factor in range(1, shard_count + 1)
            if shard_count % factor == 0 and factor * tok_rows <= max(1024, tok_rows)
        )
    )
    block_rows = grouped * tok_rows
    blocks = (
        latent_piece.reshape(-1, block_rows, latent_piece.shape[1]),
        rope_piece.reshape(-1, block_rows, rope_piece.shape[1]),
    )
    carried, _ = lax.scan(absorb, carried, blocks)
    highest, totals, accumulated = carried
    attended = (
        (accumulated / totals.T[:, :, None])
        .reshape(tok_rows, heads_here * VALUE_SIZE)
        .astype(jnp.bfloat16)
    )
    projected = jnp.dot(attended, out_weight, preferred_element_type=jnp.float32).astype(
        jnp.bfloat16
    )
    summed = lax.psum(projected, "tp").astype(jnp.float32)
    mixed_all = residual.astype(jnp.float32) + summed
    normed_all = norm_rows(mixed_all, ffn_gain).astype(jnp.bfloat16)
    mixed_own = lax.dynamic_slice_in_dim(mixed_all, tp_index * own_rows, own_rows, 0)
    gate_piece = lax.all_gather(gate_weight, "sp", axis=0, tiled=True)
    up_piece = lax.all_gather(up_weight, "sp", axis=0, tiled=True)
    gate = jnp.dot(normed_all, gate_piece, preferred_element_type=jnp.float32)
    up_part = jnp.dot(normed_all, up_piece, preferred_element_type=jnp.float32)
    hidden = (jax.nn.silu(gate) * up_part).astype(jnp.bfloat16)
    terms = jnp.dot(
        hidden,
        lax.all_gather(down_weight, "sp", axis=1, tiled=True),
        preferred_element_type=jnp.float32,
    )
    ffn_own = lax.psum_scatter(
        terms.astype(jnp.bfloat16), "tp", scatter_dimension=0, tiled=True
    ).astype(jnp.float32)
    return (mixed_own + ffn_own).astype(jnp.bfloat16)


def solution(mesh):
    return jax.shard_map(
        local,
        mesh=mesh,
        in_specs=(
            P(("grp", "sp"), "tp"),
            P(("grp", "sp"), "tp"),
            P(("grp", "sp"), None),
            P(("grp", "sp"), None),
            P(),
            P(),
            P(),
            P(("grp", "sp"), None),
            P("tp", None),
            P(),
            P("sp", "tp"),
            P("sp", "tp"),
            P("tp", "sp"),
        ),
        out_specs=P(("grp", "sp", "tp"), None),
        check_vma=False,
    )
```

profile of v0, /device:TPU:0, one launch (start us, length us, event | category | flops | bytes accessed | tf_op | source)
XLA Modules:
  0.0 180.8 jit_solution(15174663605777799072)
XLA Ops:
  0.0 0.0 copy-start
  0.0 0.8 tile.4
  0.8 0.1 copy.15
  1.0 0.8 fusion.5
  1.7 1.1 fusion.6
  2.8 1.0 fusion.8
  3.8 0.7 pad_maximum_fusion.latent
  4.6 0.0 copy-done
  4.6 1.3 fusion.4.turned
  5.9 82.0 %front.1 = (bf16[2048,384]{1,0:T(8,128)(2,1)}, bf16[2048,384]{1,0:T(8,128)(2,1)}, bf16[384,2048]{1,0:T(8,128)(2,1)}, f32[80,2048]{1,0:T(8,128)}, bf16[80,2048]{1,0:T(8,128)(2,1)}) custom-call(bf16[320,256]{1,0:T(8,128)(2,1)} %query.1, bf16[320,128]{1,0:T(8,128)(2,1)} %fusion.4.turned, bf16[320,384]{1,0:T(8,128)(2,1)} %pad_maximum_fusion.latent, ...), custom_call_target="tpu_custom_call" | custom-call | tf_op jit(solution)/shard_map/front/pallas_call | solution.py:260
  88.0 0.6 compare_convert_fusion.keep
  88.5 90.6 %spread_ffn.1 = bf16[80,2048]{1,0:T(8,128)(2,1)} custom-call(bf16[80,2048]{1,0:T(8,128)(2,1)} %get-tuple-element.10.own, bf16[2048,384]{1,0:T(8,128)(2,1)} %get-tuple-element.11.gate_w, bf16[2048,384]{1,0:T(8,128)(2,1)} %get-tuple-element.12.up_w, bf16[384,2048]{1,0:T(8,128)(2,1)} %get-tuple-element.13.down_w, f32[1,384]{1,0:T(1,128)} %compare_convert_fusion.keep, ...), custom_call_target="tpu_custom_call" | custom-call | tf_op jit(solution)/shard_map/spread_ffn/pallas_call | solution.py:435
  179.1 1.7 copy.17
  (6 shorter events, 0.0 us)
Async XLA Ops:
  0.0 4.6 %copy-start = (bf16[320,128]{1,0:T(8,128)(2,1)S(1)}, bf16[320,128]{1,0:T(8,128)(2,1)}, u32[]{:S(2)}) copy-start(bf16[320,128]{1,0:T(8,128)(2,1)} %param.14) | copy-start | bytes 245764
where the time goes:
time: 181 us
  Pallas kernels  173 us (96%)
  other arithmetic  3.43 us (2%)
  local copies, waits for them, and re-layouts  2.62 us (1%)
  matrix products  2.09 us (1%)
    pallas_call x1, Pallas kernels, spread_ffn(): pl.pallas_call(functools.partial(ffn_kernel, size), out_shape=jax.ShapeDt...  90.6 us
    pallas_call x1, Pallas kernels, front(): pl.pallas_call(functools.partial(front_kernel, size, columns), out_shape=...  82 us

commit v1 on v0

v1 whole, which is shorter than its diff:
```python
import functools

import jax
import jax.numpy as jnp
import numpy as np
from jax import lax
from jax.experimental import pallas as pl
from jax.experimental.pallas import tpu as pltpu
from jax.sharding import PartitionSpec as P

MESH = pl.DeviceIdType.MESH
UNROTATED_SIZE = 64
ROPE = 32
VALUE_SIZE = 64
GRID_W = 64


def norm_rows(values, gain):
    wide = values.astype(jnp.float32)
    return wide * lax.rsqrt(jnp.mean(wide * wide, axis=-1, keepdims=True) + 1e-06) * gain


def turn_heads(vectors, positions):
    tokens, heads, width = vectors.shape
    freqs = width // 4
    grid_pos = jnp.stack([positions // GRID_W, positions % GRID_W], axis=-1).astype(jnp.float32)
    inverse = jnp.power(10000.0, -jnp.arange(freqs, dtype=jnp.float32) / freqs)
    angles = grid_pos[:, :, None] * inverse
    cosine = jnp.cos(angles)[:, None]
    sine = jnp.sin(angles)[:, None]
    viewed = vectors.reshape(tokens, heads, 2, 2, freqs)
    first = viewed[..., 0, :]
    second = viewed[..., 1, :]
    turned = jnp.stack([first * cosine - second * sine, first * sine + second * cosine], axis=-2)
    return turned.reshape(tokens, heads, width)


def spread_hidden(token_count, hidden_columns):
    fits = lax.axis_size("tp") == 4 and lax.axis_size("grp") == 2
    return fits and 2 * token_count < 3 * hidden_columns


def column_tiles(hidden_columns):
    tiles = hidden_columns // 128
    return tiles, -(-tiles // lax.axis_size("sp"))


def window_start(at, hidden_columns):
    tiles, per = column_tiles(hidden_columns)
    return lax.div(at * (tiles - per), lax.axis_size("sp") - 1)


def signal_all(peers):
    barrier = pltpu.get_barrier_semaphore()
    for peer in peers:
        pl.semaphore_signal(barrier, inc=1, device_id=peer, device_id_type=MESH)
    pl.semaphore_wait(barrier, len(peers))


def remote(src, dst, send_sem, recv_sem, peer):
    return pltpu.make_async_remote_copy(
        src_ref=src,
        dst_ref=dst,
        send_sem=send_sem,
        recv_sem=recv_sem,
        device_id=peer,
        device_id_type=MESH,
    )


def line_order(here, size):
    table = []
    for at in range(size):
        others = [place for place in range(size) if place != at]
        flip = 1 if 2 * at < size else -1
        table.append(sorted(others, key=lambda place: (abs(place - at), (place - at) * flip)))
    columns = []
    for step in range(size - 1):
        value = jnp.int32(0)
        for at in range(size):
            value = value + jnp.where(here == at, table[at][step], 0)
        columns.append(value)
    return columns


def swap_matrix(lanes):
    freqs = ROPE // 4
    row = lax.broadcasted_iota(jnp.int32, (lanes, lanes), 0)
    lane = lax.broadcasted_iota(jnp.int32, (lanes, lanes), 1)
    first_half = lax.rem(lane, 2 * freqs) < freqs
    partner = jnp.where(first_half, lane + freqs, lane - freqs)
    sign = jnp.where(first_half, -1.0, 1.0)
    return jnp.where(row == partner, sign, 0.0).astype(jnp.bfloat16)


def layer_kernel(
    size, hidden_columns, query, query_rope, token_latent, key_rope, latent_gain, table,
    key_w, value_w, out_w, residual, gain, gate, up, down,
    out,
    gathered, keys, values, gate_v, up_v, down_v, projected, p_core, p_x,
    tokens, parts, from_core, from_x, from_z, total,
    own_sem, w_send, w_recv, y_send, y_recv,
    lz_send, lz_recv, lx_send, lx_recv, lc_send, lc_recv,
    pc_send, pc_recv, px_send, px_recv,
    z_send, z_recv, x_send, x_recv, c_send, c_recv,
    rc_send, rc_recv, rx_send, rx_recv, rz_send, rz_recv,
):
    here = lax.axis_index("sp")
    part = lax.axis_index("grp")
    t = lax.axis_index("tp")
    core = t + 1 - 2 * lax.rem(t, 2)
    across = t + 2 - 4 * lax.div(t, 2)
    diagonal = core + 2 - 4 * lax.div(core, 2)
    to_core, to_x = {"tp": core}, {"tp": across}
    depth = gate.shape[0]
    width = gate_v.shape[1]
    outer = down.shape[1]
    count = token_latent.shape[0]
    rank = token_latent.shape[1]
    rows = count // 4
    model = residual.shape[1]
    order = line_order(here, size)
    origins = [here] + order
    last = size - 1
    pending = []

    def start(*args):
        copy = remote(*args)
        copy.start()
        pending.append(copy)
        return copy

    def start_of(at):
        return pl.multiple_of(window_start(at, hidden_columns) * 128, 128)

    def piece(ref, kind, origin, half):
        if kind < 2:
            step = depth // 2
            return ref.at[pl.ds(pl.multiple_of(origin * depth + half * step, step), step), :]
        step = width // 2
        return ref.at[
            pl.ds(pl.multiple_of(half * step, step), step),
            pl.ds(pl.multiple_of(origin * outer, outer), outer),
        ]

    def source(ref, kind, target, half):
        if kind < 2:
            step = depth // 2
            return ref.at[pl.ds(pl.multiple_of(half * step, step), step), pl.ds(start_of(target), width)]
        step = width // 2
        return ref.at[pl.ds(pl.multiple_of(start_of(target) + half * step, 64), step), :]

    rope_own = key_rope[...]
    repeats = query_rope.shape[1] // ROPE
    gathered[here, :, :rank] = token_latent[...]
    gathered[here, :, rank:] = jnp.concatenate([rope_own] * repeats, axis=1)

    peers = [{"sp": lax.rem(here + shift, size)} for shift in range(1, size)]
    signal_all(peers + [to_core, to_x, {"grp": 1 - part}])

    def quarter(at):
        return pl.ds(pl.multiple_of(at * rows, rows), rows)

    lz = []
    for shift in range(1, size):
        held = gathered.at[here, quarter(t), :]
        lz.append(
            start(held, held, lz_send.at[shift - 1], lz_recv.at[shift - 1], {"sp": lax.rem(here + shift, size)})
        )
    refs = ((gate, gate_v), (up, up_v), (down, down_v))
    crossing = [[], [], []]

    def spread(kind):
        ref, held = refs[kind]
        for shift in range(1, size):
            target = lax.rem(here + shift, size)
            crossing[kind].append(
                start(
                    source(ref, kind, target, part),
                    piece(held, kind, here, part),
                    w_send.at[kind, shift - 1],
                    w_recv.at[kind, shift - 1],
                    {"sp": target},
                )
            )

    spread(0)
    spread(1)
    spread(2)
    locals_ = [[], [], []]
    for kind, (ref, held) in enumerate(refs):
        for half in range(2):
            copy = pltpu.make_async_copy(
                source(ref, kind, here, half), piece(held, kind, here, half), own_sem.at[kind, half]
            )
            copy.start()
            locals_[kind].append(copy)

    lanes = query.shape[1]
    heads = lanes // UNROTATED_SIZE
    columns = pl.ds(pl.multiple_of(t * lanes, 128), lanes)
    swap = swap_matrix(query_rope.shape[1])

    def turn(vectors, first):
        where = pl.ds(pl.multiple_of(first, 8), vectors.shape[0])
        other = jnp.dot(vectors, swap, preferred_element_type=jnp.float32)
        turned = vectors.astype(jnp.float32) * table[0, where, :] + other * table[1, where, :]
        return turned.astype(jnp.bfloat16)

    def expand(origin):
        where = pl.ds(pl.multiple_of(origin * count, count), count)
        latent = norm_rows(gathered[origin, :, :rank], latent_gain[...]).astype(jnp.bfloat16)
        keys[where, :lanes] = jnp.dot(
            latent, key_w[:, columns], preferred_element_type=jnp.float32
        ).astype(jnp.bfloat16)
        keys[where, lanes:] = turn(gathered[origin, :, rank:], origin * count)
        values[where, :] = jnp.dot(
            latent, value_w[:, columns], preferred_element_type=jnp.float32
        ).astype(jnp.bfloat16)

    turned = turn(query_rope[...], here * count)
    expand(here)
    lx, lc = {}, {}
    for shift in range(1, size):
        origin = lax.rem(here - shift + size, size)
        lz[shift - 1].wait_recv()
        held = gathered.at[origin, quarter(t), :]
        lx[shift] = start(held, held, lx_send.at[shift - 1], lx_recv.at[shift - 1], to_x)
        lc[shift] = start(held, held, lc_send.at[shift - 1, 0], lc_recv.at[shift - 1, 0], to_core)
    lc_second = {}
    for shift in range(1, size):
        origin = lax.rem(here - shift + size, size)
        lx[shift].wait_recv()
        held = gathered.at[origin, quarter(across), :]
        lc_second[shift] = start(held, held, lc_send.at[shift - 1, 1], lc_recv.at[shift - 1, 1], to_core)
    for shift in range(1, size):
        lc[shift].wait_recv()
        lc_second[shift].wait_recv()
        expand(lax.rem(here - shift + size, size))

    scale = (UNROTATED_SIZE + ROPE) ** (-0.5)
    lane = lax.broadcasted_iota(jnp.int32, (1, lanes), 1)
    rope_lane = lax.broadcasted_iota(jnp.int32, (1, turned.shape[1]), 1)
    attended = jnp.zeros((count, lanes), jnp.float32)
    for head in range(heads):
        mine = (lane >= head * UNROTATED_SIZE) & (lane < (head + 1) * UNROTATED_SIZE)
        rope_mine = (rope_lane >= head * ROPE) & (rope_lane < (head + 1) * ROPE)
        both = jnp.concatenate(
            [
                jnp.where(mine, query[...].astype(jnp.float32), 0.0),
                jnp.where(rope_mine, turned.astype(jnp.float32), 0.0),
            ],
            axis=1,
        ).astype(jnp.bfloat16)
        scores = (
            lax.dot_general(
                both, keys[...], (((1,), (1,)), ((), ())), preferred_element_type=jnp.float32
            )
            * scale
        )
        raised = jnp.exp(scores - jnp.max(scores, axis=1, keepdims=True))
        totals = jnp.sum(raised, axis=1, keepdims=True)
        weighted = jnp.dot(
            raised.astype(jnp.bfloat16), values[...], preferred_element_type=jnp.float32
        )
        attended = jnp.where(mine, weighted / totals, attended)
    attended = attended.astype(jnp.bfloat16)
    step = 512
    for col in range(0, model, step):
        term = jnp.dot(attended, out_w[:, col : col + step], preferred_element_type=jnp.float32)
        projected[:, :, col : col + step] = term.astype(jnp.bfloat16).reshape(4, rows, step)

    def plus(one, two):
        return one.astype(jnp.float32) + two.astype(jnp.float32)

    pc_first = start(projected.at[diagonal], p_core.at[1], pc_send.at[1], pc_recv.at[1], to_core)
    pc_second = start(projected.at[core], p_core.at[0], pc_send.at[0], pc_recv.at[0], to_core)
    pc_first.wait_recv()
    projected[across] = plus(projected[across], p_core[1]).astype(jnp.bfloat16)
    px = start(projected.at[across], p_x, px_send, px_recv, to_x)

    swaps = [[], [], []]

    def forward(kind):
        held_ref = refs[kind][1]
        for shift in range(1, size):
            origin = lax.rem(here - shift + size, size)
            crossing[kind][shift - 1].wait_recv()
            held = piece(held_ref, kind, origin, part)
            swaps[kind].append(
                start(held, held, y_send.at[kind, shift - 1], y_recv.at[kind, shift - 1], {"grp": 1 - part})
            )

    def settle(kind):
        for copy in locals_[kind]:
            copy.wait()
        for copy in swaps[kind]:
            copy.wait_recv()

    pc_second.wait_recv()
    total[...] = residual[quarter(t), :].astype(jnp.float32) + plus(projected[t], p_core[0])
    forward(0)
    px.wait_recv()
    mixed = total[...] + p_x[...].astype(jnp.float32)
    total[...] = mixed
    tokens[here, t] = (
        mixed * lax.rsqrt(jnp.mean(mixed * mixed, axis=1, keepdims=True) + 1e-06) * gain[...]
    ).astype(jnp.bfloat16)

    own_block = tokens.at[here, t]

    def own_copy(way):
        target = here + 1 - 2 * way
        return remote(own_block, own_block, z_send.at[way], z_recv.at[here], {"sp": target})

    @pl.when(here < last)
    def _():
        own_copy(0).start()

    @pl.when(here > 0)
    def _():
        own_copy(1).start()

    def passing(i):
        origin = origins[i]
        block = tokens.at[origin, t]
        target = jnp.where(origin < here, here + 1, here - 1)
        valid = (target >= 0) & (target <= last)
        target = jnp.clip(target, 0, last)
        return valid, remote(block, block, z_send.at[1 + i], z_recv.at[origin], {"sp": target})

    x_copies, c_first, c_second, r_first, r_second, rx, rz = {}, {}, {}, {}, {}, {}, {}

    def step_a(i):
        o = origins[i]
        block = tokens.at[o, t]
        if i:
            remote(block, block, z_send.at[1 + i], z_recv.at[o], to_x).wait_recv()
            valid, copy = passing(i)
            pl.when(valid)(copy.start)
        x_copies[i] = start(block, block, x_send.at[i], x_recv.at[i], to_x)
        c_first[i] = start(block, block, c_send.at[i, 0], c_recv.at[i, 0], to_core)

    def step_b(i):
        x_copies[i].wait_recv()
        block = tokens.at[origins[i], across]
        c_second[i] = start(block, block, c_send.at[i, 1], c_recv.at[i, 1], to_core)

    tiles, per = column_tiles(hidden_columns)
    before = jnp.where(here > 0, window_start(jnp.maximum(here - 1, 0), hidden_columns) + per, 0)
    first = (before - window_start(here, hidden_columns)) * 128
    keep = lax.broadcasted_iota(jnp.int32, (1, width), 1) >= first

    def step_c(i):
        o = origins[i]
        c_first[i].wait_recv()
        c_second[i].wait_recv()
        if i == 0:
            settle(0)
            settle(1)
        x = tokens[o].reshape(4 * rows, model)
        gated = jnp.dot(x, gate_v[...], preferred_element_type=jnp.float32)
        lifted = jnp.dot(x, up_v[...], preferred_element_type=jnp.float32)
        hidden = jnp.where(keep, gated / (1.0 + jnp.exp(-gated)) * lifted, 0.0).astype(jnp.bfloat16)
        if i == 0:
            forward(2)
            settle(2)
        for col in range(0, model, step):
            term = jnp.dot(hidden, down_v[:, col : col + step], preferred_element_type=jnp.float32)
            parts[o, :, :, col : col + step] = term.astype(jnp.bfloat16).reshape(4, rows, step)
        r_first[i] = start(parts.at[o, diagonal], from_core.at[i, 1], rc_send.at[i, 1], rc_recv.at[i, 1], to_core)
        r_second[i] = start(parts.at[o, core], from_core.at[i, 0], rc_send.at[i, 0], rc_recv.at[i, 0], to_core)

    def step_d(i):
        o = origins[i]
        r_first[i].wait_recv()
        parts[o, across] = plus(parts[o, across], from_core[i, 1]).astype(jnp.bfloat16)
        rx[i] = start(parts.at[o, across], from_x.at[i], rx_send.at[i], rx_recv.at[i], to_x)
        r_second[i].wait_recv()
        parts[o, t] = plus(parts[o, t], from_core[i, 0]).astype(jnp.bfloat16)

    def step_e(i):
        o = origins[i]
        rx[i].wait_recv()
        if i == 0:
            total[...] = total[...] + plus(parts[o, t], from_x[i])
            return
        parts[o, t] = plus(parts[o, t], from_x[i]).astype(jnp.bfloat16)
        rz[i] = start(parts.at[o, t], from_z.at[here], rz_send.at[i], rz_recv.at[here], {"sp": o})

    steps = {"a": step_a, "b": step_b, "c": step_c, "d": step_d, "e": step_e}
    step_a(0)
    forward(1)
    sequence = []
    for i in range(size + 1):
        for name, lag in (("a", -1), ("b", 0), ("c", 0), ("d", 0), ("e", 1)):
            if 0 <= i - lag <= last and (name, i - lag) != ("a", 0):
                sequence.append((name, i - lag))
    for name, i in sequence:
        steps[name](i)
    result = total[...]
    for i in range(1, size):
        o = origins[i]
        remote(from_z.at[o], from_z.at[o], rz_send.at[i], rz_recv.at[o], to_x).wait_recv()
        result = result + from_z[o].astype(jnp.float32)
    out[...] = result.astype(out.dtype)

    @pl.when(here < last)
    def _():
        own_copy(0).wait_send()

    @pl.when(here > 0)
    def _():
        own_copy(1).wait_send()

    for i in range(1, size):
        valid, copy = passing(i)
        pl.when(valid)(copy.wait_send)
    for copy in pending:
        copy.wait_send()


def position_table(token_count, lanes):
    freqs = ROPE // 4
    lane = np.arange(lanes)
    place = np.arange(token_count)
    inverse = np.power(10000.0, -(lane % freqs).astype(np.float64) / freqs)
    grid = np.where((lane % ROPE < ROPE // 2)[None], (place // GRID_W)[:, None], (place % GRID_W)[:, None])
    angles = grid.astype(np.float64) * inverse[None]
    return np.stack([np.cos(angles), np.sin(angles)]).astype(np.float32)


def spread_layer(
    query_nope, query_rope, token_latent, key_rope, latent_norm_gain, key_w, value_w,
    residual, out_w, ffn_gain, gate_w, up_w, down_w,
):
    size = lax.axis_size("sp")
    depth, columns = gate_w.shape
    width = column_tiles(columns)[1] * 128
    count, model = residual.shape
    lanes = query_nope.shape[1]
    wide = token_latent.shape[1] + query_rope.shape[1]
    block = (count // 4, model)
    table = jnp.asarray(position_table(size * count, query_rope.shape[1]))
    dma = pltpu.SemaphoreType.DMA
    narrow = jnp.bfloat16
    vmem = lambda *lead: pltpu.VMEM(lead + block, narrow)
    line = [dma((size - 1,)), dma((size - 1,))]
    line_pair = [dma((size - 1, 2)), dma((size - 1, 2))]
    pieces = [dma((3, size - 1)), dma((3, size - 1))]
    single = [dma((size,)), dma((size,))]
    double = [dma((size, 2)), dma((size, 2))]
    here = pl.BlockSpec(memory_space=pltpu.VMEM)
    away = pl.BlockSpec(memory_space=pl.ANY)
    return pl.pallas_call(
        functools.partial(layer_kernel, size, columns),
        out_shape=jax.ShapeDtypeStruct(block, narrow),
        in_specs=[here] * 11 + [away] * 3,
        out_specs=here,
        scratch_shapes=[
            pltpu.VMEM((size, count, wide), narrow),
            pltpu.VMEM((size * count, lanes + query_rope.shape[1]), narrow),
            pltpu.VMEM((size * count, lanes), narrow),
            pltpu.VMEM((size * depth, width), narrow),
            pltpu.VMEM((size * depth, width), narrow),
            pltpu.VMEM((width, size * down_w.shape[1]), narrow),
            vmem(4), vmem(2), vmem(),
            vmem(size, 4), vmem(size, 4), vmem(size, 2), vmem(size), vmem(size),
            pltpu.VMEM(block, jnp.float32),
            dma((3, 2)), *pieces, *pieces,
            *line, *line, *line_pair,
            dma((2,)), dma((2,)), dma, dma,
            dma((size + 1,)), dma((size,)), *single, *double, *double, *single, *single,
        ],
        compiler_params=pltpu.CompilerParams(collective_id=0, has_side_effects=True),
        name="layer",
    )(
        query_nope, query_rope, token_latent, key_rope, latent_norm_gain[None], table,
        key_w, value_w, out_w, residual, ffn_gain[None], gate_w, up_w, down_w,
    )


def local(
    query_nope,
    query_rope,
    token_latent,
    key_rope,
    latent_norm_gain,
    key_expand_weight,
    value_expand_weight,
    residual,
    out_weight,
    ffn_gain,
    gate_weight,
    up_weight,
    down_weight,
):
    if spread_hidden(query_nope.shape[0] * lax.axis_size("sp"), gate_weight.shape[1]):
        return spread_layer(
            query_nope,
            query_rope,
            token_latent,
            key_rope,
            latent_norm_gain,
            key_expand_weight,
            value_expand_weight,
            residual,
            out_weight,
            ffn_gain,
            gate_weight,
            up_weight,
            down_weight,
        )
    tok_rows = query_nope.shape[0]
    heads_here = query_nope.shape[1] // UNROTATED_SIZE
    own_rows = tok_rows // lax.axis_size("tp")
    tp_index = lax.axis_index("tp")
    positions = lax.axis_index("sp") * tok_rows + jnp.arange(tok_rows, dtype=jnp.int32)
    query_flat = query_nope.reshape(tok_rows, heads_here, UNROTATED_SIZE)
    query_turned = turn_heads(
        query_rope.astype(jnp.float32).reshape(tok_rows, heads_here, ROPE), positions
    ).astype(jnp.bfloat16)
    latent = norm_rows(token_latent, latent_norm_gain).astype(jnp.bfloat16)
    key_turned = turn_heads(key_rope.astype(jnp.float32)[:, None, :], positions)[:, 0].astype(
        jnp.bfloat16
    )
    key_cols = lax.dynamic_slice_in_dim(
        key_expand_weight, tp_index * heads_here * UNROTATED_SIZE, heads_here * UNROTATED_SIZE, 1
    )
    value_cols = lax.dynamic_slice_in_dim(
        value_expand_weight, tp_index * heads_here * VALUE_SIZE, heads_here * VALUE_SIZE, 1
    )
    score_scale = (UNROTATED_SIZE + ROPE) ** (-0.5)

    def absorb(carried, block_in):
        latent_block, rope_block = block_in
        block_rows = latent_block.shape[0]
        key_rows = jnp.dot(latent_block, key_cols, preferred_element_type=jnp.float32).astype(
            jnp.bfloat16
        )
        key_rows = key_rows.reshape(block_rows, heads_here, UNROTATED_SIZE)
        value_rows = jnp.dot(latent_block, value_cols, preferred_element_type=jnp.float32).astype(
            jnp.bfloat16
        )
        value_rows = value_rows.reshape(block_rows, heads_here, VALUE_SIZE)
        scores = (
            jnp.einsum("qhd,khd->hqk", query_flat, key_rows, preferred_element_type=jnp.float32)
            + jnp.einsum(
                "qhd,kd->hqk", query_turned, rope_block, preferred_element_type=jnp.float32
            )
        ) * score_scale
        highest, totals, accumulated = carried
        new_highest = jnp.maximum(highest, jnp.max(scores, axis=-1))
        shrink = jnp.exp(highest - new_highest)
        weights = jnp.exp(scores - new_highest[:, :, None])
        totals = totals * shrink + jnp.sum(weights, axis=-1)
        accumulated = accumulated * shrink.T[:, :, None] + jnp.einsum(
            "hqk,khd->qhd",
            weights.astype(jnp.bfloat16),
            value_rows,
            preferred_element_type=jnp.float32,
        )
        return ((new_highest, totals, accumulated), None)

    initial = (
        jnp.full((heads_here, tok_rows), -jnp.inf, jnp.float32),
        jnp.zeros((heads_here, tok_rows), jnp.float32),
        jnp.zeros((tok_rows, heads_here, VALUE_SIZE), jnp.float32),
    )
    carried = initial
    latent_piece = lax.all_gather(latent, "sp", axis=0, tiled=True)
    rope_piece = lax.all_gather(key_turned, "sp", axis=0, tiled=True)
    shard_count = latent_piece.shape[0] // tok_rows
    grouped = max(
        (
            factor
            for factor in range(1, shard_count + 1)
            if shard_count % factor == 0 and factor * tok_rows <= max(1024, tok_rows)
        )
    )
    block_rows = grouped * tok_rows
    blocks = (
        latent_piece.reshape(-1, block_rows, latent_piece.shape[1]),
        rope_piece.reshape(-1, block_rows, rope_piece.shape[1]),
    )
    carried, _ = lax.scan(absorb, carried, blocks)
    highest, totals, accumulated = carried
    attended = (
        (accumulated / totals.T[:, :, None])
        .reshape(tok_rows, heads_here * VALUE_SIZE)
        .astype(jnp.bfloat16)
    )
    projected = jnp.dot(attended, out_weight, preferred_element_type=jnp.float32).astype(
        jnp.bfloat16
    )
    summed = lax.psum(projected, "tp").astype(jnp.float32)
    mixed_all = residual.astype(jnp.float32) + summed
    normed_all = norm_rows(mixed_all, ffn_gain).astype(jnp.bfloat16)
    mixed_own = lax.dynamic_slice_in_dim(mixed_all, tp_index * own_rows, own_rows, 0)
    gate_piece = lax.all_gather(gate_weight, "sp", axis=0, tiled=True)
    up_piece = lax.all_gather(up_weight, "sp", axis=0, tiled=True)
    gate = jnp.dot(normed_all, gate_piece, preferred_element_type=jnp.float32)
    up_part = jnp.dot(normed_all, up_piece, preferred_element_type=jnp.float32)
    hidden = (jax.nn.silu(gate) * up_part).astype(jnp.bfloat16)
    terms = jnp.dot(
        hidden,
        lax.all_gather(down_weight, "sp", axis=1, tiled=True),
        preferred_element_type=jnp.float32,
    )
    ffn_own = lax.psum_scatter(
        terms.astype(jnp.bfloat16), "tp", scatter_dimension=0, tiled=True
    ).astype(jnp.float32)
    return (mixed_own + ffn_own).astype(jnp.bfloat16)


def solution(mesh):
    return jax.shard_map(
        local,
        mesh=mesh,
        in_specs=(
            P(("grp", "sp"), "tp"),
            P(("grp", "sp"), "tp"),
            P(("grp", "sp"), None),
            P(("grp", "sp"), None),
            P(),
            P(),
            P(),
            P(("grp", "sp"), None),
            P("tp", None),
            P(),
            P("sp", "tp"),
            P("sp", "tp"),
            P("tp", "sp"),
        ),
        out_specs=P(("grp", "sp", "tp"), None),
        check_vma=False,
    )
```

time: 181 us -> 151 us (0.83)
  Pallas kernels: 173 us -> 147 us
  other arithmetic: 3.43 us -> 0 us
  matrix products: 2.09 us -> 0 us
    pallas_call x2 -> x1, Pallas kernels: 173 us -> 147 us  [spread_layer(): pl.pallas_call(functools.partial(layer_kernel, size, columns), out_shape=...]
    dot_general x2 -> x0, matrix products: 2.09 us -> none  [turn_lanes(): other = jnp.dot(vectors, swap, preferred_element_type=jnp.float32)]
where the time goes in v1:
time: 151 us
  Pallas kernels  147 us (97%)
  local copies, waits for them, and re-layouts  3.19 us (2%)
    pallas_call x1, Pallas kernels, spread_layer(): pl.pallas_call(functools.partial(layer_kernel, size, columns), out_shape=...  147 us
    unnamed x2, local copies, waits for them, and re-layouts  3.19 us

profile of v1, /device:TPU:0, one launch (start us, length us, event | category | flops | bytes accessed | tf_op | source)
XLA Modules:
  0.0 150.6 jit_solution(9523536480454432803)
XLA Ops:
  0.0 1.5 copy.15.key_rope
  1.5 147.3 %layer.1 = bf16[80,2048]{1,0:T(8,128)(2,1)} custom-call(bf16[320,256]{1,0:T(8,128)(2,1)} %query.1, bf16[320,128]{1,0:T(8,128)(2,1)} %query_rope.1, bf16[320,256]{1,0:T(8,128)(2,1)} %token_latent.1, bf16[320,32]{1,0:T(8,128)(2,1)} %copy.15.key_rope, f32[1,256]{1,0:T(1,128)} %bitcast.3, f32[2,1280,128]{2,1,0:T(8,128)} %constant.2.clone.table, ...), custom_call_target="tpu_custom_call" | custom-call | tf_op jit(solution)/shard_map/layer/pallas_call | solution.py:455
  148.8 1.7 %copy.17 = bf16[80,2048]{1,0:T(8,128)(2,1)} copy(bf16[80,2048]{1,0:T(8,128)(2,1)} %layer.1) | data formatting | bytes 655360

commit v2 on v1

--- a/solution.py
+++ b/solution.py
@@ -94,12 +94,12 @@
 
 
 def layer_kernel(
-    size, hidden_columns, query, query_rope, token_latent, key_rope, latent_gain, table,
-    key_w, value_w, out_w, residual, gain, gate, up, down,
+    size, hidden_columns, query, query_rope, token_latent, key_rope, latent_gain,
+    key_all, value_all, out_all, residual_all, table_all, gain, gate, up, down,
     out,
-    gathered, keys, values, gate_v, up_v, down_v, projected, p_core, p_x,
-    tokens, parts, from_core, from_x, from_z, total,
-    own_sem, w_send, w_recv, y_send, y_recv,
+    key_w, value_w, out_w, residual, table, gathered, keys, values, gate_v, up_v, down_v, projected, p_core, p_x,
+    tokens, parts, hidden, from_core, from_x, from_z, total,
+    in_sem, own_sem, w_send, w_recv, y_send, y_recv,
     lz_send, lz_recv, lx_send, lx_recv, lc_send, lc_recv,
     pc_send, pc_recv, px_send, px_recv,
     z_send, z_recv, x_send, x_recv, c_send, c_recv,
@@ -119,6 +119,9 @@
     rank = token_latent.shape[1]
     rows = count // 4
     model = residual.shape[1]
+    lanes = query.shape[1]
+    columns = pl.ds(pl.multiple_of(t * lanes, 128), lanes)
+    step = outer
     order = line_order(here, size)
     origins = [here] + order
     last = size - 1
@@ -150,16 +153,31 @@
         step = width // 2
         return ref.at[pl.ds(pl.multiple_of(start_of(target) + half * step, 64), step), :]
 
+    def quarter(at):
+        return pl.ds(pl.multiple_of(at * rows, rows), rows)
+
+    loads = [
+        pltpu.make_async_copy(src, dst, in_sem.at[n])
+        for n, (src, dst) in enumerate(
+            (
+                (table_all, table),
+                (key_all.at[:, columns], key_w),
+                (value_all.at[:, columns], value_w),
+                (out_all, out_w),
+                (residual_all.at[quarter(t), :], residual),
+            )
+        )
+    ]
+    for copy in loads:
+        copy.start()
     rope_own = key_rope[...]
     repeats = query_rope.shape[1] // ROPE
     gathered[here, :, :rank] = token_latent[...]
     gathered[here, :, rank:] = jnp.concatenate([rope_own] * repeats, axis=1)
 
     peers = [{"sp": lax.rem(here + shift, size)} for shift in range(1, size)]
-    signal_all(peers + [to_core, to_x, {"grp": 1 - part}])
-
-    def quarter(at):
-        return pl.ds(pl.multiple_of(at * rows, rows), rows)
+    with jax.named_scope('barrier'):
+        signal_all(peers + [to_core, to_x, {"grp": 1 - part}])
 
     lz = []
     for shift in range(1, size):
@@ -184,9 +202,6 @@
                 )
             )
 
-    spread(0)
-    spread(1)
-    spread(2)
     locals_ = [[], [], []]
     for kind, (ref, held) in enumerate(refs):
         for half in range(2):
@@ -196,9 +211,7 @@
             copy.start()
             locals_[kind].append(copy)
 
-    lanes = query.shape[1]
     heads = lanes // UNROTATED_SIZE
-    columns = pl.ds(pl.multiple_of(t * lanes, 128), lanes)
     swap = swap_matrix(query_rope.shape[1])
 
     def turn(vectors, first):
@@ -211,85 +224,97 @@
         where = pl.ds(pl.multiple_of(origin * count, count), count)
         latent = norm_rows(gathered[origin, :, :rank], latent_gain[...]).astype(jnp.bfloat16)
         keys[where, :lanes] = jnp.dot(
-            latent, key_w[:, columns], preferred_element_type=jnp.float32
+            latent, key_w[...], preferred_element_type=jnp.float32
         ).astype(jnp.bfloat16)
         keys[where, lanes:] = turn(gathered[origin, :, rank:], origin * count)
         values[where, :] = jnp.dot(
-            latent, value_w[:, columns], preferred_element_type=jnp.float32
+            latent, value_w[...], preferred_element_type=jnp.float32
         ).astype(jnp.bfloat16)
 
-    turned = turn(query_rope[...], here * count)
-    expand(here)
+    for copy in loads[:3]:
+        copy.wait()
+    with jax.named_scope('own_kv'):
+        turned = turn(query_rope[...], here * count)
+        expand(here)
     lx, lc = {}, {}
     for shift in range(1, size):
         origin = lax.rem(here - shift + size, size)
-        lz[shift - 1].wait_recv()
+        with jax.named_scope('lat_z'):
+            lz[shift - 1].wait_recv()
         held = gathered.at[origin, quarter(t), :]
         lx[shift] = start(held, held, lx_send.at[shift - 1], lx_recv.at[shift - 1], to_x)
         lc[shift] = start(held, held, lc_send.at[shift - 1, 0], lc_recv.at[shift - 1, 0], to_core)
+    spread(0)
+    spread(1)
     lc_second = {}
     for shift in range(1, size):
         origin = lax.rem(here - shift + size, size)
-        lx[shift].wait_recv()
+        with jax.named_scope('lat_x'):
+            lx[shift].wait_recv()
         held = gathered.at[origin, quarter(across), :]
         lc_second[shift] = start(held, held, lc_send.at[shift - 1, 1], lc_recv.at[shift - 1, 1], to_core)
     for shift in range(1, size):
         lc[shift].wait_recv()
-        lc_second[shift].wait_recv()
-        expand(lax.rem(here - shift + size, size))
+        with jax.named_scope('lat_c'):
+            lc_second[shift].wait_recv()
+        with jax.named_scope('expand'):
+            expand(lax.rem(here - shift + size, size))
 
     scale = (UNROTATED_SIZE + ROPE) ** (-0.5)
     lane = lax.broadcasted_iota(jnp.int32, (1, lanes), 1)
     rope_lane = lax.broadcasted_iota(jnp.int32, (1, turned.shape[1]), 1)
     attended = jnp.zeros((count, lanes), jnp.float32)
-    for head in range(heads):
-        mine = (lane >= head * UNROTATED_SIZE) & (lane < (head + 1) * UNROTATED_SIZE)
-        rope_mine = (rope_lane >= head * ROPE) & (rope_lane < (head + 1) * ROPE)
-        both = jnp.concatenate(
-            [
-                jnp.where(mine, query[...].astype(jnp.float32), 0.0),
-                jnp.where(rope_mine, turned.astype(jnp.float32), 0.0),
-            ],
-            axis=1,
-        ).astype(jnp.bfloat16)
-        scores = (
-            lax.dot_general(
-                both, keys[...], (((1,), (1,)), ((), ())), preferred_element_type=jnp.float32
+    with jax.named_scope('heads'):
+        for head in range(heads):
+            mine = (lane >= head * UNROTATED_SIZE) & (lane < (head + 1) * UNROTATED_SIZE)
+            rope_mine = (rope_lane >= head * ROPE) & (rope_lane < (head + 1) * ROPE)
+            both = jnp.concatenate(
+                [
+                    jnp.where(mine, query[...].astype(jnp.float32), 0.0),
+                    jnp.where(rope_mine, turned.astype(jnp.float32), 0.0),
+                ],
+                axis=1,
+            ).astype(jnp.bfloat16)
+            scores = (
+                lax.dot_general(
+                    both, keys[...], (((1,), (1,)), ((), ())), preferred_element_type=jnp.float32
+                )
+                * scale
             )
-            * scale
-        )
-        raised = jnp.exp(scores - jnp.max(scores, axis=1, keepdims=True))
-        totals = jnp.sum(raised, axis=1, keepdims=True)
-        weighted = jnp.dot(
-            raised.astype(jnp.bfloat16), values[...], preferred_element_type=jnp.float32
-        )
-        attended = jnp.where(mine, weighted / totals, attended)
+            raised = jnp.exp(scores - jnp.max(scores, axis=1, keepdims=True))
+            totals = jnp.sum(raised, axis=1, keepdims=True)
+            weighted = jnp.dot(
+                raised.astype(jnp.bfloat16), values[...], preferred_element_type=jnp.float32
+            )
+            attended = jnp.where(mine, weighted / totals, attended)
     attended = attended.astype(jnp.bfloat16)
-    step = 512
-    for col in range(0, model, step):
-        term = jnp.dot(attended, out_w[:, col : col + step], preferred_element_type=jnp.float32)
-        projected[:, :, col : col + step] = term.astype(jnp.bfloat16).reshape(4, rows, step)
+    for copy in loads[3:]:
+        copy.wait()
+    with jax.named_scope('proj'):
+        for col in range(0, model, step):
+            term = jnp.dot(attended, out_w[:, col : col + step], preferred_element_type=jnp.float32)
+            projected[:, :, col : col + step] = term.astype(jnp.bfloat16).reshape(4, rows, step)
 
     def plus(one, two):
         return one.astype(jnp.float32) + two.astype(jnp.float32)
 
     pc_first = start(projected.at[diagonal], p_core.at[1], pc_send.at[1], pc_recv.at[1], to_core)
     pc_second = start(projected.at[core], p_core.at[0], pc_send.at[0], pc_recv.at[0], to_core)
-    pc_first.wait_recv()
+    with jax.named_scope('pc1'):
+        pc_first.wait_recv()
     projected[across] = plus(projected[across], p_core[1]).astype(jnp.bfloat16)
     px = start(projected.at[across], p_x, px_send, px_recv, to_x)
 
     swaps = [[], [], []]
 
-    def forward(kind):
-        held_ref = refs[kind][1]
-        for shift in range(1, size):
-            origin = lax.rem(here - shift + size, size)
+    def forward(kind, shift):
+        origin = lax.rem(here - shift + size, size)
+        with jax.named_scope(f"cross{kind}_{shift}"):
             crossing[kind][shift - 1].wait_recv()
-            held = piece(held_ref, kind, origin, part)
-            swaps[kind].append(
-                start(held, held, y_send.at[kind, shift - 1], y_recv.at[kind, shift - 1], {"grp": 1 - part})
-            )
+        held = piece(refs[kind][1], kind, origin, part)
+        swaps[kind].append(
+            start(held, held, y_send.at[kind, shift - 1], y_recv.at[kind, shift - 1], {"grp": 1 - part})
+        )
 
     def settle(kind):
         for copy in locals_[kind]:
@@ -297,10 +322,13 @@
         for copy in swaps[kind]:
             copy.wait_recv()
 
-    pc_second.wait_recv()
-    total[...] = residual[quarter(t), :].astype(jnp.float32) + plus(projected[t], p_core[0])
-    forward(0)
-    px.wait_recv()
+    with jax.named_scope('pc2'):
+        pc_second.wait_recv()
+    total[...] = residual[...].astype(jnp.float32) + plus(projected[t], p_core[0])
+    for item in ('01',):
+        forward(0, int(item[1]))
+    with jax.named_scope('px'):
+        px.wait_recv()
     mixed = total[...] + p_x[...].astype(jnp.float32)
     total[...] = mixed
     tokens[here, t] = (
@@ -329,20 +357,22 @@
         target = jnp.clip(target, 0, last)
         return valid, remote(block, block, z_send.at[1 + i], z_recv.at[origin], {"sp": target})
 
-    x_copies, c_first, c_second, r_first, r_second, rx, rz = {}, {}, {}, {}, {}, {}, {}
+    x_copies, c_first, c_second, r_first, r_second, rx = {}, {}, {}, {}, {}, {}
 
     def step_a(i):
         o = origins[i]
         block = tokens.at[o, t]
         if i:
-            remote(block, block, z_send.at[1 + i], z_recv.at[o], to_x).wait_recv()
+            with jax.named_scope(f'tokz{i}'):
+                remote(block, block, z_send.at[1 + i], z_recv.at[o], to_x).wait_recv()
             valid, copy = passing(i)
             pl.when(valid)(copy.start)
         x_copies[i] = start(block, block, x_send.at[i], x_recv.at[i], to_x)
         c_first[i] = start(block, block, c_send.at[i, 0], c_recv.at[i, 0], to_core)
 
     def step_b(i):
-        x_copies[i].wait_recv()
+        with jax.named_scope(f'tokx{i}'):
+            x_copies[i].wait_recv()
         block = tokens.at[origins[i], across]
         c_second[i] = start(block, block, c_send.at[i, 1], c_recv.at[i, 1], to_core)
 
@@ -354,56 +384,71 @@
     def step_c(i):
         o = origins[i]
         c_first[i].wait_recv()
-        c_second[i].wait_recv()
+        with jax.named_scope(f'tokc{i}'):
+            c_second[i].wait_recv()
         if i == 0:
-            settle(0)
-            settle(1)
+            with jax.named_scope('settle01'):
+                settle(0)
+                settle(1)
         x = tokens[o].reshape(4 * rows, model)
-        gated = jnp.dot(x, gate_v[...], preferred_element_type=jnp.float32)
-        lifted = jnp.dot(x, up_v[...], preferred_element_type=jnp.float32)
-        hidden = jnp.where(keep, gated / (1.0 + jnp.exp(-gated)) * lifted, 0.0).astype(jnp.bfloat16)
-        if i == 0:
-            forward(2)
-            settle(2)
-        for col in range(0, model, step):
-            term = jnp.dot(hidden, down_v[:, col : col + step], preferred_element_type=jnp.float32)
-            parts[o, :, :, col : col + step] = term.astype(jnp.bfloat16).reshape(4, rows, step)
-        r_first[i] = start(parts.at[o, diagonal], from_core.at[i, 1], rc_send.at[i, 1], rc_recv.at[i, 1], to_core)
-        r_second[i] = start(parts.at[o, core], from_core.at[i, 0], rc_send.at[i, 0], rc_recv.at[i, 0], to_core)
-
-    def step_d(i):
-        o = origins[i]
-        r_first[i].wait_recv()
-        parts[o, across] = plus(parts[o, across], from_core[i, 1]).astype(jnp.bfloat16)
-        rx[i] = start(parts.at[o, across], from_x.at[i], rx_send.at[i], rx_recv.at[i], to_x)
-        r_second[i].wait_recv()
-        parts[o, t] = plus(parts[o, t], from_core[i, 0]).astype(jnp.bfloat16)
-
-    def step_e(i):
-        o = origins[i]
-        rx[i].wait_recv()
-        if i == 0:
-            total[...] = total[...] + plus(parts[o, t], from_x[i])
-            return
-        parts[o, t] = plus(parts[o, t], from_x[i]).astype(jnp.bfloat16)
-        rz[i] = start(parts.at[o, t], from_z.at[here], rz_send.at[i], rz_recv.at[here], {"sp": o})
-
-    steps = {"a": step_a, "b": step_b, "c": step_c, "d": step_d, "e": step_e}
-    step_a(0)
-    forward(1)
-    sequence = []
-    for i in range(size + 1):
-        for name, lag in (("a", -1), ("b", 0), ("c", 0), ("d", 0), ("e", 1)):
-            if 0 <= i - lag <= last and (name, i - lag) != ("a", 0):
-                sequence.append((name, i - lag))
-    for name, i in sequence:
-        steps[name](i)
-    result = total[...]
-    for i in range(1, size):
-        o = origins[i]
-        remote(from_z.at[o], from_z.at[o], rz_send.at[i], rz_recv.at[o], to_x).wait_recv()
-        result = result + from_z[o].astype(jnp.float32)
-    out[...] = result.astype(out.dtype)
+        with jax.named_scope(f'gateup{i}'):
+            gated = jnp.dot(x, gate_v[...], preferred_element_type=jnp.float32)
+            lifted = jnp.dot(x, up_v[...], preferred_element_type=jnp.float32)
+            fired = jnp.where(keep, gated / (1.0 + jnp.exp(-gated)) * lifted, 0.0).astype(jnp.bfloat16)
+        hidden[o] = fired
+
+    def step_f(j):
+        origin = lax.rem(here - j + size, size)
+        if j:
+            with jax.named_scope(f"settle2_{j}"):
+                swaps[2][j - 1].wait_recv()
+        else:
+            for copy in locals_[2]:
+                copy.wait()
+        fired = hidden[...].reshape(size * count, width)
+        with jax.named_scope(f"downmm{j}"):
+            held = pl.ds(pl.multiple_of(origin * outer, outer), outer)
+            term = jnp.dot(fired, down_v[:, held], preferred_element_type=jnp.float32)
+            parts[j] = term.astype(jnp.bfloat16).reshape(size, 4, rows, outer)
+        r_first[j] = start(parts.at[j, :, diagonal], from_core.at[j, 1], rc_send.at[j, 1], rc_recv.at[j, 1], to_core)
+        r_second[j] = start(parts.at[j, :, core], from_core.at[j, 0], rc_send.at[j, 0], rc_recv.at[j, 0], to_core)
+
+    def step_d(j):
+        with jax.named_scope(f"rc1_{j}"):
+            r_first[j].wait_recv()
+        parts[j, :, across] = plus(parts[j, :, across], from_core[j, 1]).astype(jnp.bfloat16)
+        rx[j] = start(parts.at[j, :, across], from_x.at[j], rx_send.at[j], rx_recv.at[j], to_x)
+        with jax.named_scope(f"rc2_{j}"):
+            r_second[j].wait_recv()
+        parts[j, :, t] = plus(parts[j, :, t], from_core[j, 0]).astype(jnp.bfloat16)
+
+    def step_e(j):
+        origin = lax.rem(here - j + size, size)
+        with jax.named_scope(f"rx{j}"):
+            rx[j].wait_recv()
+        for i in range(size - 1, 0, -1):
+            o = origins[i]
+            parts[j, o, t] = plus(parts[j, o, t], from_x[j, o]).astype(jnp.bfloat16)
+            start(parts.at[j, o, t], from_z.at[origin, here], rz_send.at[j, i], rz_recv.at[origin, here], {"sp": o})
+        held = pl.ds(pl.multiple_of(origin * outer, outer), outer)
+        total[:, held] = total[:, held] + plus(parts[j, here, t], from_x[j, here])
+
+    steps = {
+        "a": step_a, "b": step_b, "c": step_c, "d": step_d, "e": step_e, "f": step_f,
+        "0": lambda shift: forward(0, shift), "1": lambda shift: forward(1, shift),
+        "2": lambda shift: forward(2, shift), "s": spread,
+    }
+    for item in ('a0', '02', '03', '11', '12', '13', 'a1', 'b0', 'a2', 'c0', 'b1', 'a3', 's2', 'c1', 'b2', 'c2', 'b3', 'c3', 'f0', '21', 'd0', '22', 'f1', '23', 'd1', 'e0', 'f2', 'd2', 'e1', 'f3', 'd3', 'e2', 'e3'):
+        steps[item[0]](int(item[1]))
+    for place in range(size):
+        held = slice(place * outer, (place + 1) * outer)
+        result = total[:, held]
+        for i in range(1, size):
+            o = origins[i]
+            with jax.named_scope(f"rz{place}_{i}"):
+                remote(from_z.at[place, o], from_z.at[place, o], rz_send.at[0, i], rz_recv.at[place, o], to_x).wait_recv()
+            result = result + from_z[place, o].astype(jnp.float32)
+        out[:, held] = result.astype(out.dtype)
 
     @pl.when(here < last)
     def _():
@@ -445,6 +490,8 @@
     dma = pltpu.SemaphoreType.DMA
     narrow = jnp.bfloat16
     vmem = lambda *lead: pltpu.VMEM(lead + block, narrow)
+    slab = lambda *lead: pltpu.VMEM(lead + (block[0], down_w.shape[1]), narrow)
+    square = [dma((size, size)), dma((size, size))]
     line = [dma((size - 1,)), dma((size - 1,))]
     line_pair = [dma((size - 1, 2)), dma((size - 1, 2))]
     pieces = [dma((3, size - 1)), dma((3, size - 1))]
@@ -455,9 +502,14 @@
     return pl.pallas_call(
         functools.partial(layer_kernel, size, columns),
         out_shape=jax.ShapeDtypeStruct(block, narrow),
-        in_specs=[here] * 11 + [away] * 3,
+        in_specs=[here] * 5 + [away] * 5 + [here] + [away] * 3,
         out_specs=here,
         scratch_shapes=[
+            pltpu.VMEM((key_w.shape[0], lanes), narrow),
+            pltpu.VMEM((value_w.shape[0], lanes), narrow),
+            pltpu.VMEM(out_w.shape, narrow),
+            vmem(),
+            pltpu.VMEM(table.shape, jnp.float32),
             pltpu.VMEM((size, count, wide), narrow),
             pltpu.VMEM((size * count, lanes + query_rope.shape[1]), narrow),
             pltpu.VMEM((size * count, lanes), narrow),
@@ -465,18 +517,19 @@
             pltpu.VMEM((size * depth, width), narrow),
             pltpu.VMEM((width, size * down_w.shape[1]), narrow),
             vmem(4), vmem(2), vmem(),
-            vmem(size, 4), vmem(size, 4), vmem(size, 2), vmem(size), vmem(size),
+            vmem(size, 4), slab(size, size, 4), pltpu.VMEM((size, count, width), narrow),
+            slab(size, 2, size), slab(size, size), slab(size, size),
             pltpu.VMEM(block, jnp.float32),
-            dma((3, 2)), *pieces, *pieces,
+            dma((5,)), dma((3, 2)), *pieces, *pieces,
             *line, *line, *line_pair,
             dma((2,)), dma((2,)), dma, dma,
-            dma((size + 1,)), dma((size,)), *single, *double, *double, *single, *single,
+            dma((size + 1,)), dma((size,)), *single, *double, *double, *single, *square,
         ],
         compiler_params=pltpu.CompilerParams(collective_id=0, has_side_effects=True),
         name="layer",
     )(
-        query_nope, query_rope, token_latent, key_rope, latent_norm_gain[None], table,
-        key_w, value_w, out_w, residual, ffn_gain[None], gate_w, up_w, down_w,
+        query_nope, query_rope, token_latent, key_rope, latent_norm_gain[None],
+        key_w, value_w, out_w, residual, table, ffn_gain[None], gate_w, up_w, down_w,
     )
 
 

time: 151 us -> 127 us (0.84)
  Pallas kernels: 147 us -> 123 us
    pallas_call x1, Pallas kernels: 147 us -> 123 us  [spread_layer(): pl.pallas_call(functools.partial(layer_kernel, size, columns), out_shape=...]
where the time goes in v2:
time: 127 us; the launch traced here: 126 us
  Pallas kernels  123 us (97%)
  local copies, waits for them, and re-layouts  3.19 us (3%)
    pallas_call x1, Pallas kernels, spread_layer(): pl.pallas_call(functools.partial(layer_kernel, size, columns), out_shape=...  123 us
    unnamed x2, local copies, waits for them, and re-layouts  3.19 us

profile of v2, /device:TPU:0, one launch (start us, length us, event | category | flops | bytes accessed | tf_op | source)
XLA Modules:
  0.0 126.3 jit_solution(16341513724893324023)
XLA Ops:
  0.0 1.5 %copy.15.key_rope = bf16[320,32]{1,0:T(8,128)(2,1)} copy(bf16[320,32]{0,1:T(8,128)(2,1)} %param.17) | data formatting | bytes 40960 | tf_op args[3]
  1.5 123.1 %layer.1 = bf16[80,2048]{1,0:T(8,128)(2,1)} custom-call(bf16[320,256]{1,0:T(8,128)(2,1)} %query.1, bf16[320,128]{1,0:T(8,128)(2,1)} %query_rope.1, bf16[320,256]{1,0:T(8,128)(2,1)} %token_latent.1, bf16[320,32]{1,0:T(8,128)(2,1)} %copy.15.key_rope, f32[1,256]{1,0:T(1,128)} %bitcast.3, bf16[256,1024]{1,0:T(8,128)(2,1)} %key_all.1, ...), custom_call_target="tpu_custom_call" | custom-call | tf_op jit(solution)/shard_map/layer/pallas_call | solution.py:502
  124.6 1.7 %copy.17 = bf16[80,2048]{1,0:T(8,128)(2,1)} copy(bf16[80,2048]{1,0:T(8,128)(2,1)} %layer.1) | data formatting | bytes 655360

commit v3 on v2

--- a/solution.py
+++ b/solution.py
@@ -45,9 +45,35 @@
     return tiles, -(-tiles // lax.axis_size("sp"))
 
 
-def window_start(at, hidden_columns):
+def window_start(at, parity, hidden_columns):
     tiles, per = column_tiles(hidden_columns)
-    return lax.div(at * (tiles - per), lax.axis_size("sp") - 1)
+    from_left = jnp.minimum(at * per, tiles - per)
+    from_right = jnp.maximum(tiles - (lax.axis_size("sp") - at) * per, 0)
+    return jnp.where(parity == 0, from_left, from_right)
+
+
+class Either:
+    def __init__(self, small_out, small_in, make):
+        self.small_out, self.small_in, self.make = small_out, small_in, make
+
+    def run(self, small, name):
+        for value, chosen in ((False, jnp.logical_not(small)), (True, small)):
+
+            @pl.when(chosen)
+            def _():
+                getattr(self.make(value), name)()
+
+    def start(self):
+        self.run(self.small_out, "start")
+
+    def wait_send(self):
+        self.run(self.small_out, "wait_send")
+
+    def wait_recv(self):
+        self.run(self.small_in, "wait_recv")
+
+    def wait(self):
+        self.run(self.small_out, "wait")
 
 
 def signal_all(peers):
@@ -133,25 +159,47 @@
         pending.append(copy)
         return copy
 
+    parity = lax.rem(t, 2)
+    tiles, per = column_tiles(hidden_columns)
+    spare = (size * per - tiles) * 128
+    inset = pl.multiple_of((1 - parity) * spare, 128)
+    narrow = width - spare
+
+    def small(at):
+        return at == (1 - parity) * last
+
     def start_of(at):
-        return pl.multiple_of(window_start(at, hidden_columns) * 128, 128)
-
-    def piece(ref, kind, origin, half):
+        return pl.multiple_of(window_start(at, parity, hidden_columns) * 128, 128)
+
+    def piece(ref, kind, origin, half, short):
         if kind < 2:
             step = depth // 2
-            return ref.at[pl.ds(pl.multiple_of(origin * depth + half * step, step), step), :]
-        step = width // 2
+            where = pl.ds(pl.multiple_of(origin * depth + half * step, step), step)
+            return ref.at[where, pl.ds(inset, narrow) if short else pl.ds(0, width)]
+        step = (narrow if short else width) // 2
+        first = half * step + (inset if short else 0)
         return ref.at[
-            pl.ds(pl.multiple_of(half * step, step), step),
+            pl.ds(pl.multiple_of(first, 64), step),
             pl.ds(pl.multiple_of(origin * outer, outer), outer),
         ]
 
-    def source(ref, kind, target, half):
+    def source(ref, kind, target, half, short):
+        first = start_of(target) + (inset if short else 0)
         if kind < 2:
             step = depth // 2
-            return ref.at[pl.ds(pl.multiple_of(half * step, step), step), pl.ds(start_of(target), width)]
-        step = width // 2
-        return ref.at[pl.ds(pl.multiple_of(start_of(target) + half * step, 64), step), :]
+            return ref.at[
+                pl.ds(pl.multiple_of(half * step, step), step),
+                pl.ds(pl.multiple_of(first, 128), narrow if short else width),
+            ]
+        step = (narrow if short else width) // 2
+        return ref.at[pl.ds(pl.multiple_of(first + half * step, 64), step), :]
+
+    if spare:
+
+        @pl.when(small(here))
+        def _():
+            unused = pl.ds(pl.multiple_of(parity * narrow, 128), spare)
+            down_v[unused, :] = jnp.zeros((spare, size * outer), down_v.dtype)
 
     def quarter(at):
         return pl.ds(pl.multiple_of(at * rows, rows), rows)
@@ -188,26 +236,54 @@
     refs = ((gate, gate_v), (up, up_v), (down, down_v))
     crossing = [[], [], []]
 
+    def weight_copy(kind, shift):
+        ref, held = refs[kind]
+        target = lax.rem(here + shift, size)
+        return Either(
+            small(target),
+            small(here),
+            lambda short: remote(
+                source(ref, kind, target, part, short),
+                piece(held, kind, here, part, short),
+                w_send.at[kind, shift - 1],
+                w_recv.at[kind, shift - 1],
+                {"sp": target},
+            ),
+        )
+
+    def own_weight(kind, half):
+        ref, held = refs[kind]
+        return Either(
+            small(here),
+            small(here),
+            lambda short: pltpu.make_async_copy(
+                source(ref, kind, here, half, short),
+                piece(held, kind, here, half, short),
+                own_sem.at[kind, half],
+            ),
+        )
+
+    def swap_copy(kind, shift):
+        origin = lax.rem(here - shift + size, size)
+
+        def make(short):
+            held = piece(refs[kind][1], kind, origin, part, short)
+            return remote(
+                held, held, y_send.at[kind, shift - 1], y_recv.at[kind, shift - 1], {"grp": 1 - part}
+            )
+
+        return Either(small(here), small(here), make)
+
     def spread(kind):
-        ref, held = refs[kind]
         for shift in range(1, size):
-            target = lax.rem(here + shift, size)
-            crossing[kind].append(
-                start(
-                    source(ref, kind, target, part),
-                    piece(held, kind, here, part),
-                    w_send.at[kind, shift - 1],
-                    w_recv.at[kind, shift - 1],
-                    {"sp": target},
-                )
-            )
+            crossing[kind].append(weight_copy(kind, shift))
+            crossing[kind][-1].start()
+        pending.extend(crossing[kind])
 
     locals_ = [[], [], []]
-    for kind, (ref, held) in enumerate(refs):
+    for kind in range(3):
         for half in range(2):
-            copy = pltpu.make_async_copy(
-                source(ref, kind, here, half), piece(held, kind, here, half), own_sem.at[kind, half]
-            )
+            copy = own_weight(kind, half)
             copy.start()
             locals_[kind].append(copy)
 
@@ -308,13 +384,12 @@
     swaps = [[], [], []]
 
     def forward(kind, shift):
-        origin = lax.rem(here - shift + size, size)
         with jax.named_scope(f"cross{kind}_{shift}"):
             crossing[kind][shift - 1].wait_recv()
-        held = piece(refs[kind][1], kind, origin, part)
-        swaps[kind].append(
-            start(held, held, y_send.at[kind, shift - 1], y_recv.at[kind, shift - 1], {"grp": 1 - part})
-        )
+        copy = swap_copy(kind, shift)
+        copy.start()
+        pending.append(copy)
+        swaps[kind].append(copy)
 
     def settle(kind):
         for copy in locals_[kind]:
@@ -376,10 +451,10 @@
         block = tokens.at[origins[i], across]
         c_second[i] = start(block, block, c_send.at[i, 1], c_recv.at[i, 1], to_core)
 
-    tiles, per = column_tiles(hidden_columns)
-    before = jnp.where(here > 0, window_start(jnp.maximum(here - 1, 0), hidden_columns) + per, 0)
-    first = (before - window_start(here, hidden_columns)) * 128
-    keep = lax.broadcasted_iota(jnp.int32, (1, width), 1) >= first
+    column = lax.broadcasted_iota(jnp.int32, (1, width), 1)
+    first_kept = jnp.where(small(here), inset, 0)
+    kept = jnp.where(small(here), narrow, width)
+    keep = (column >= first_kept) & (column < first_kept + kept)
 
     def step_c(i):
         o = origins[i]

time: 127 us -> 125 us (0.984)
  Pallas kernels: 123 us -> 120 us
    pallas_call x1, Pallas kernels: 123 us -> 120 us  [spread_layer(): pl.pallas_call(functools.partial(layer_kernel, size, columns), out_shape=...]
where the time goes in v3:
time: 125 us; the launch traced here: 124 us
  Pallas kernels  120 us (96%)
  local copies, waits for them, and re-layouts  3.19 us (3%)
    pallas_call x1, Pallas kernels, spread_layer(): pl.pallas_call(functools.partial(layer_kernel, size, columns), out_shape=...  120 us
    unnamed x2, local copies, waits for them, and re-layouts  3.19 us

profile of v3, /device:TPU:0, one launch (start us, length us, event | category | flops | bytes accessed | tf_op | source)
XLA Modules:
  0.0 123.5 jit_solution(4010033821616237290)
XLA Ops:
  0.0 1.5 %copy.15.key_rope = bf16[320,32]{1,0:T(8,128)(2,1)} copy(bf16[320,32]{0,1:T(8,128)(2,1)} %param.17) | data formatting | bytes 40960 | tf_op args[3]
  1.5 120.3 %layer.1 = bf16[80,2048]{1,0:T(8,128)(2,1)} custom-call(bf16[320,256]{1,0:T(8,128)(2,1)} %query.1, bf16[320,128]{1,0:T(8,128)(2,1)} %query_rope.1, bf16[320,256]{1,0:T(8,128)(2,1)} %token_latent.1, bf16[320,32]{1,0:T(8,128)(2,1)} %copy.15.key_rope, f32[1,256]{1,0:T(1,128)} %bitcast.3, bf16[256,1024]{1,0:T(8,128)(2,1)} %key_all.1, ...), custom_call_target="tpu_custom_call" | custom-call | tf_op jit(solution)/shard_map/layer/pallas_call | solution.py:577
  121.8 1.7 %copy.17 = bf16[80,2048]{1,0:T(8,128)(2,1)} copy(bf16[80,2048]{1,0:T(8,128)(2,1)} %layer.1) | data formatting | bytes 655360

commit v4 on v3

--- a/solution.py
+++ b/solution.py
@@ -492,19 +492,24 @@
         with jax.named_scope(f"rc1_{j}"):
             r_first[j].wait_recv()
         parts[j, :, across] = plus(parts[j, :, across], from_core[j, 1]).astype(jnp.bfloat16)
-        rx[j] = start(parts.at[j, :, across], from_x.at[j], rx_send.at[j], rx_recv.at[j], to_x)
+        for i in range(size - 1, -1, -1):
+            o = origins[i]
+            rx[j, i] = start(
+                parts.at[j, o, across], from_x.at[j, o], rx_send.at[j, i], rx_recv.at[j, i], to_x
+            )
         with jax.named_scope(f"rc2_{j}"):
             r_second[j].wait_recv()
         parts[j, :, t] = plus(parts[j, :, t], from_core[j, 0]).astype(jnp.bfloat16)
 
     def step_e(j):
         origin = lax.rem(here - j + size, size)
-        with jax.named_scope(f"rx{j}"):
-            rx[j].wait_recv()
         for i in range(size - 1, 0, -1):
             o = origins[i]
+            with jax.named_scope(f"rx{j}"):
+                rx[j, i].wait_recv()
             parts[j, o, t] = plus(parts[j, o, t], from_x[j, o]).astype(jnp.bfloat16)
             start(parts.at[j, o, t], from_z.at[origin, here], rz_send.at[j, i], rz_recv.at[origin, here], {"sp": o})
+        rx[j, 0].wait_recv()
         held = pl.ds(pl.multiple_of(origin * outer, outer), outer)
         total[:, held] = total[:, held] + plus(parts[j, here, t], from_x[j, here])
 
@@ -598,7 +603,7 @@
             dma((5,)), dma((3, 2)), *pieces, *pieces,
             *line, *line, *line_pair,
             dma((2,)), dma((2,)), dma, dma,
-            dma((size + 1,)), dma((size,)), *single, *double, *double, *single, *square,
+            dma((size + 1,)), dma((size,)), *single, *double, *double, *square, *square,
         ],
         compiler_params=pltpu.CompilerParams(collective_id=0, has_side_effects=True),
         name="layer",

time: 125 us -> 121 us (0.968)
  Pallas kernels: 120 us -> 116 us
    pallas_call x1, Pallas kernels: 120 us -> 116 us  [spread_layer(): pl.pallas_call(functools.partial(layer_kernel, size, columns), out_shape=...]
where the time goes in v4:
time: 121 us; the launch traced here: 119 us
  Pallas kernels  116 us (96%)
  local copies, waits for them, and re-layouts  3.19 us (3%)
    pallas_call x1, Pallas kernels, spread_layer(): pl.pallas_call(functools.partial(layer_kernel, size, columns), out_shape=...  116 us
    unnamed x2, local copies, waits for them, and re-layouts  3.19 us

profile of v4, /device:TPU:0, one launch (start us, length us, event | category | flops | bytes accessed | tf_op | source)
XLA Modules:
  0.0 119.4 jit_solution(17108243039277709090)
XLA Ops:
  0.0 1.5 %copy.15.key_rope = bf16[320,32]{1,0:T(8,128)(2,1)} copy(bf16[320,32]{0,1:T(8,128)(2,1)} %param.17) | data formatting | bytes 40960 | tf_op args[3]
  1.5 116.2 %layer.1 = bf16[80,2048]{1,0:T(8,128)(2,1)} custom-call(bf16[320,256]{1,0:T(8,128)(2,1)} %query.1, bf16[320,128]{1,0:T(8,128)(2,1)} %query_rope.1, bf16[320,256]{1,0:T(8,128)(2,1)} %token_latent.1, bf16[320,32]{1,0:T(8,128)(2,1)} %copy.15.key_rope, f32[1,256]{1,0:T(1,128)} %bitcast.3, bf16[256,1024]{1,0:T(8,128)(2,1)} %key_all.1, ...), custom_call_target="tpu_custom_call" | custom-call | tf_op jit(solution)/shard_map/layer/pallas_call | solution.py:582
  117.7 1.7 %copy.17 = bf16[80,2048]{1,0:T(8,128)(2,1)} copy(bf16[80,2048]{1,0:T(8,128)(2,1)} %layer.1) | data formatting | bytes 655360
